TPU v7x, 32 devices: a whole 2x2x4 slice. The times are simulated.
32 devices in a mesh: grp: 2 (over y), ep: 4 (over z), tp: 4 (over x, core).
Axes of the slice: x: 2, y: 2, z: 4, core: 2. Of those that a mesh axis runs over, the one named last changes fastest.
Arguments:
- tokens: bfloat16 [2048, 2048], P(('grp', 'ep'), 'tp'), parts along dimension 0, may hold values from -6 to 6
- norm_gain: float32 [2048], replicated, may hold values from 0.1 to 1.9
- expert_ids: int32 [2048, 2], P(('grp', 'ep')), parts along dimension 0, may hold values from 0 to 3, all different within a row; in each aligned block of 256 rows (0 to 255, 256 to 511, ...) at most 192 rows name the same one
- gate_weights: float32 [2048, 2], P(('grp', 'ep')), parts along dimension 0, may hold values from 0.25 to 1
- w_gate: bfloat16 [4, 2048, 3072], P('ep', None, 'tp'), may hold values from -0.125 to 0.125
- w_up: bfloat16 [4, 2048, 3072], P('ep', None, 'tp'), may hold values from -0.125 to 0.125
- w_down: bfloat16 [4, 3072, 2048], P('ep', 'tp'), may hold values from -0.15625 to 0.15625
Outputs:
- mixed: bfloat16 [2048, 2048], P(('grp', 'ep'), 'tp'), parts along dimension 0
There are 2 independent parts, one for each index of `grp`. A program takes and returns all parts, laid end to end along the dimension named above; an argument that names none is the same for every part. Nothing has to cross between parts.
Inputs may be any that keep to these rules, and one draw needn't show every extreme that they name: `expert_ids`: each token names 2 different experts. Within the 256 rows of one index of ep (aligned blocks) no expert is named more than 192 times, and in some blocks one expert is named exactly 192 times.
All inputs are finite; a program needn't handle non-finite values.
Results may differ from a plain program's by a relative error of at most 0.015.
Values may be sent and summed in bfloat16 or wider, within the bound.
A program may use at most 64 MiB of HBM per device.

v0:
```python
import functools

import jax
import jax.numpy as jnp
from jax import lax
from jax.experimental import pallas as pl
from jax.experimental.pallas import tpu as pltpu
from jax.sharding import PartitionSpec as P

epsilon = 1e-06
AHEAD = 2
LAG = 1
MESH = pl.DeviceIdType.MESH


def nearest_first(count):
    table = []
    for e in range(count):
        mirrored = 1 if 2 * e < count else -1
        table.append(sorted(range(count), key=lambda s: (abs(s - e), mirrored * s)))
    return table


def look_up(table, row, column):
    value = jnp.int32(0)
    for r, entries in enumerate(table):
        for c, entry in enumerate(entries):
            value = jnp.where((row == r) & (column == c), entry, value)
    return value


def layer_kernel(
    n_ep,
    cap,
    cuts,
    tok_ref,
    ids_ref,
    gate_ref,
    gain_ref,
    wg_ref,
    wu_ref,
    wd_ref,
    out_ref,
    wg,
    wu,
    wd,
    packed,
    rows,
    normed,
    hidden,
    own,
    to_core,
    from_core,
    to_chip,
    from_chip,
    result,
    back,
    w_sem,
    z_send,
    z_recv,
    x_send,
    x_recv,
    d_send,
    d_recv,
    e_send,
    e_recv,
    pc_send,
    pc_recv,
    px_send,
    px_recv,
    r_send,
    r_recv,
):
    tok_count, col_count = tok_ref.shape
    top_count = ids_ref.shape[0]
    n_tp = rows.shape[1]
    width = n_tp * col_count
    ep = lax.axis_index("ep")
    tp = lax.axis_index("tp")
    core = tp % 2
    sibling = tp + 1 - 2 * core
    across = (tp + 2) % n_tp
    side = tp // 2
    table = nearest_first(n_ep)
    order = [look_up(table, ep, i) for i in range(n_ep)]

    weights = [
        pltpu.make_async_copy(wg_ref.at[0], wg, w_sem.at[0]),
        pltpu.make_async_copy(wu_ref.at[0], wu, w_sem.at[1]),
    ]
    piece_of = [
        (1 - side) * 2 + 1 - core,
        side * 2 + 1 - core,
        (1 - side) * 2 + core,
        side * 2 + core,
    ]
    for j, piece in enumerate(piece_of):
        cols = pl.ds(pl.multiple_of(piece * col_count, col_count), col_count)
        weights.append(
            pltpu.make_async_copy(wd_ref.at[0, :, cols], wd.at[j], w_sem.at[2 + j])
        )
    for copy in weights:
        copy.start()

    barrier = pltpu.get_barrier_semaphore()
    for step in range(1, n_ep):
        pl.semaphore_signal(
            barrier, inc=1, device_id={"ep": (ep + step) % n_ep}, device_id_type=MESH
        )
    for peer in (sibling, across):
        pl.semaphore_signal(barrier, inc=1, device_id={"tp": peer}, device_id_type=MESH)

    lane = lax.broadcasted_iota(jnp.int32, (tok_count, 128), 1)
    lane_expert = jnp.full((tok_count, 128), -1, jnp.int32)
    for i in range(n_ep):
        lane_expert = jnp.where(lane == i, order[i], lane_expert)
    ids = ids_ref[...].astype(jnp.float32).T
    gates = gate_ref[...].T
    lane_expert = lane_expert.astype(jnp.float32)
    named = jnp.zeros((tok_count, 128), jnp.float32)
    weight = jnp.zeros((tok_count, 128), jnp.float32)
    for k in range(top_count):
        hit = ids[:, k : k + 1] == lane_expert
        named = named + jnp.where(hit, 1.0, 0.0)
        weight = weight + jnp.where(hit, gates[:, k : k + 1], 0.0)
    before = jnp.where(
        lax.broadcasted_iota(jnp.int32, (tok_count, tok_count), 1)
        < lax.broadcasted_iota(jnp.int32, (tok_count, tok_count), 0),
        1.0,
        0.0,
    ).astype(jnp.bfloat16)
    place = jnp.dot(before, named.astype(jnp.bfloat16), preferred_element_type=jnp.float32)
    place = jnp.where(named > 0.0, place, -1.0)
    place_t = place.T
    slot_rows = lax.broadcasted_iota(jnp.int32, (cap, tok_count), 0).astype(jnp.float32)

    def pack(i):
        pick = jnp.where(slot_rows == place_t[i : i + 1, :], 1.0, 0.0).astype(jnp.bfloat16)
        return jnp.dot(pick, tok_ref[...], preferred_element_type=jnp.float32).astype(
            jnp.bfloat16
        )

    def z_copy(here, there, h):
        return pltpu.make_async_remote_copy(
            src_ref=packed.at[there * cuts + h],
            dst_ref=rows.at[here * cuts + h, tp],
            send_sem=z_send.at[there * cuts + h],
            recv_sem=z_recv.at[here * cuts + h],
            device_id={"ep": there},
            device_id_type=MESH,
        )

    def x_copy(i):
        return pltpu.make_async_remote_copy(
            src_ref=rows.at[i, tp],
            dst_ref=rows.at[i, tp],
            send_sem=x_send.at[i],
            recv_sem=x_recv.at[i],
            device_id={"tp": across},
            device_id_type=MESH,
        )

    def d_copy(i):
        return pltpu.make_async_remote_copy(
            src_ref=rows.at[i, tp],
            dst_ref=rows.at[i, tp],
            send_sem=d_send.at[i],
            recv_sem=d_recv.at[i],
            device_id={"tp": sibling},
            device_id_type=MESH,
        )

    def e_copy(i):
        return pltpu.make_async_remote_copy(
            src_ref=rows.at[i, across],
            dst_ref=rows.at[i, across],
            send_sem=e_send.at[i],
            recv_sem=e_recv.at[i],
            device_id={"tp": sibling},
            device_id_type=MESH,
        )

    def pc_copy(i, j):
        return pltpu.make_async_remote_copy(
            src_ref=to_core.at[i, j],
            dst_ref=from_core.at[i, j],
            send_sem=pc_send.at[i, j],
            recv_sem=pc_recv.at[i, j],
            device_id={"tp": sibling},
            device_id_type=MESH,
        )

    def px_copy(i):
        return pltpu.make_async_remote_copy(
            src_ref=to_chip.at[i],
            dst_ref=from_chip.at[i],
            send_sem=px_send.at[i],
            recv_sem=px_recv.at[i],
            device_id={"tp": across},
            device_id_type=MESH,
        )

    def r_copy(here, there, h):
        return pltpu.make_async_remote_copy(
            src_ref=result.at[there * cuts + h],
            dst_ref=back.at[here * cuts + h],
            send_sem=r_send.at[there * cuts + h],
            recv_sem=r_recv.at[here * cuts + h],
            device_id={"ep": there},
            device_id_type=MESH,
        )

    piece_rows = cap // cuts
    stages = n_ep * cuts
    values = pack(1)
    for h in range(cuts):
        packed[order[1] * cuts + h] = values[h * piece_rows : (h + 1) * piece_rows]
    values = pack(0)
    for h in range(cuts):
        rows[ep * cuts + h, tp] = values[h * piece_rows : (h + 1) * piece_rows]
    pl.semaphore_wait(barrier, n_ep + 1)
    for h in range(cuts):
        z_copy(ep, order[1], h).start()
        x_copy(ep * cuts + h).start()
        d_copy(ep * cuts + h).start()
    for i in range(2, n_ep):
        values = pack(i)
        for h in range(cuts):
            packed[order[i] * cuts + h] = values[h * piece_rows : (h + 1) * piece_rows]
            z_copy(ep, order[i], h).start()
    for copy in weights:
        copy.wait()

    def unit_of(i):
        return look_up(table, ep, i // cuts) * cuts + i % cuts

    def finish(i):
        s = unit_of(i)
        pc_copy(s, 1).wait_recv()
        total = own[i % (LAG + 1)] + from_core[s, 1].astype(jnp.float32)
        px_copy(s).wait_recv()
        total = total + from_chip[s].astype(jnp.float32)
        result[s] = total.astype(jnp.bfloat16)

        @pl.when(i >= cuts)
        def _():
            r_copy(ep, s // cuts, s % cuts).start()

    def forward(i):
        s = unit_of(i)
        z_copy(s // cuts, s // cuts, s % cuts).wait_recv()
        x_copy(s).start()
        d_copy(s).start()

    for i in range(cuts, AHEAD):
        forward(i)
    x_copy(unit_of(0)).wait_recv()
    e_copy(unit_of(0)).start()

    def stage(i, carry):
        s = unit_of(i)
        d_copy(s).wait_recv()
        e_copy(s).wait_recv()
        square_sum = jnp.zeros((piece_rows, 1), jnp.float32)
        for k in range(n_tp):
            part = rows[s, k].astype(jnp.float32)
            square_sum = square_sum + jnp.sum(part * part, axis=1, keepdims=True)
        factor = lax.rsqrt(square_sum / width + epsilon)
        for k in range(n_tp):
            cols = slice(k * col_count, (k + 1) * col_count)
            part = rows[s, k].astype(jnp.float32)
            normed[:, cols] = (part * factor * gain_ref[:, cols]).astype(jnp.bfloat16)
        gate_part = jnp.dot(normed[...], wg[...], preferred_element_type=jnp.float32)
        up_part = jnp.dot(normed[...], wu[...], preferred_element_type=jnp.float32)
        hidden[...] = (gate_part / (1.0 + jnp.exp(-gate_part)) * up_part).astype(jnp.bfloat16)
        @pl.when((i + AHEAD >= cuts) & (i + AHEAD < stages))
        def _():
            forward(i + AHEAD)

        @pl.when(i + 1 < stages)
        def _():
            after = unit_of(i + 1)
            x_copy(after).wait_recv()
            e_copy(after).start()

        for j in range(2):
            to_core[s, j] = jnp.dot(
                hidden[...], wd[j], preferred_element_type=jnp.float32
            ).astype(jnp.bfloat16)
            pc_copy(s, j).start()
        part = jnp.dot(hidden[...], wd[2], preferred_element_type=jnp.float32)
        own[i % (LAG + 1)] = jnp.dot(hidden[...], wd[3], preferred_element_type=jnp.float32)
        pc_copy(s, 0).wait_recv()
        to_chip[s] = (part + from_core[s, 0].astype(jnp.float32)).astype(jnp.bfloat16)
        px_copy(s).start()

        @pl.when(i >= LAG)
        def _():
            finish(i - LAG)

        return carry

    lax.fori_loop(0, stages, stage, 0)
    for i in range(stages - LAG, stages):
        finish(i)

    slot_lanes = lax.broadcasted_iota(jnp.int32, (tok_count, piece_rows), 1).astype(
        jnp.float32
    )
    mixed = jnp.zeros((tok_count, col_count), jnp.float32)
    for i in range(n_ep):
        taken = jnp.zeros((tok_count, col_count), jnp.float32)
        for h in range(cuts):
            pick = jnp.where(slot_lanes + h * piece_rows == place[:, i : i + 1], 1.0, 0.0)
            unit = order[i] * cuts + h
            if i == 0:
                values = result[unit]
            else:
                r_copy(order[i], order[i], h).wait_recv()
                values = back[unit]
            taken = taken + jnp.dot(
                pick.astype(jnp.bfloat16), values, preferred_element_type=jnp.float32
            )
        mixed = mixed + weight[:, i : i + 1] * taken
    out_ref[...] = mixed.astype(jnp.bfloat16)

    for i in range(1, n_ep):
        for h in range(cuts):
            z_copy(ep, order[i], h).wait_send()
            r_copy(ep, order[i], h).wait_send()
    for i in range(stages):
        x_copy(i).wait_send()
        d_copy(i).wait_send()
        e_copy(i).wait_send()
        pc_copy(i, 0).wait_send()
        pc_copy(i, 1).wait_send()
        px_copy(i).wait_send()


def fused(tokens, norm_gain, expert_ids, gate_weights, w_gate, w_up, w_down):
    tok_count, col_count = tokens.shape
    top_count = expert_ids.shape[1]
    n_ep = lax.axis_size("ep")
    n_tp = lax.axis_size("tp")
    cap = 3 * tok_count * top_count // (2 * n_ep)
    cuts = 2 if cap % 32 == 0 else 1
    stages, piece_rows = n_ep * cuts, cap // cuts
    width = norm_gain.shape[0]
    units = w_gate.shape[2]
    bf16 = jnp.bfloat16
    vmem = pl.BlockSpec(memory_space=pltpu.VMEM)
    anywhere = pl.BlockSpec(memory_space=pl.ANY)
    sems = pltpu.SemaphoreType.DMA
    return pl.pallas_call(
        functools.partial(layer_kernel, n_ep, cap, cuts),
        out_shape=jax.ShapeDtypeStruct((tok_count, col_count), bf16),
        in_specs=[vmem] * 4 + [anywhere] * 3,
        out_specs=vmem,
        scratch_shapes=[
            pltpu.VMEM((width, units), bf16),
            pltpu.VMEM((width, units), bf16),
            pltpu.VMEM((n_tp, units, col_count), bf16),
            pltpu.VMEM((stages, piece_rows, col_count), bf16),
            pltpu.VMEM((stages, n_tp, piece_rows, col_count), bf16),
            pltpu.VMEM((piece_rows, width), bf16),
            pltpu.VMEM((piece_rows, units), bf16),
            pltpu.VMEM((LAG + 1, piece_rows, col_count), jnp.float32),
            pltpu.VMEM((stages, 2, piece_rows, col_count), bf16),
            pltpu.VMEM((stages, 2, piece_rows, col_count), bf16),
        ]
        + [pltpu.VMEM((stages, piece_rows, col_count), bf16)] * 4
        + [sems((2 + n_tp,))]
        + [sems((stages,))] * 8
        + [sems((stages, 2))] * 2
        + [sems((stages,))] * 4,
        compiler_params=pltpu.CompilerParams(
            collective_id=0, has_side_effects=True, vmem_limit_bytes=56 * 2**20
        ),
    )(
        tokens,
        expert_ids.T,
        gate_weights.T,
        norm_gain.reshape(1, width),
        w_gate,
        w_up,
        w_down,
    )


def on_device(tokens, norm_gain, expert_ids, gate_weights, w_gate, w_up, w_down):
    tok_count = tokens.shape[0]
    top_count = expert_ids.shape[1]
    expert_count = lax.axis_size("ep")
    capacity = 3 * tok_count * top_count // (2 * expert_count)
    model_width = norm_gain.shape[0]
    flat_ids = expert_ids.reshape(-1)
    onehot = (flat_ids[:, None] == jnp.arange(expert_count, dtype=jnp.int32)[None, :]).astype(
        jnp.int32
    )
    earlier = jnp.cumsum(onehot, axis=0) - onehot
    slot_index = jnp.sum(earlier * onehot, axis=1)
    dest_index = flat_ids * capacity + slot_index
    owner_index = jnp.arange(tok_count * top_count, dtype=jnp.int32) // top_count
    slot_token = (
        jnp.full((expert_count * capacity,), tok_count, jnp.int32).at[dest_index].set(owner_index)
    )
    tok_values = tokens.astype(jnp.float32)
    square_sum = lax.psum(jnp.sum(tok_values * tok_values, axis=1, keepdims=True), "tp")
    col_count = tokens.shape[1]
    gain_part = lax.dynamic_slice_in_dim(norm_gain, lax.axis_index("tp") * col_count, col_count)
    normed = (tok_values * lax.rsqrt(square_sum / model_width + epsilon) * gain_part).astype(
        jnp.bfloat16
    )
    buffer = jnp.take(normed, slot_token, axis=0, mode="fill", fill_value=0).reshape(
        expert_count, capacity, -1
    )
    received = lax.all_to_all(buffer, "ep", split_axis=0, concat_axis=0, tiled=True)
    source_count, item_count, col_count = received.shape
    tok_rows = received.reshape(-1, col_count)
    col_piece = lax.all_gather(tok_rows, "tp", axis=1, tiled=True)
    gate_rows = w_gate[0]
    up_rows = w_up[0]
    gate_part = jnp.dot(col_piece, gate_rows, preferred_element_type=jnp.float32)
    up_part = jnp.dot(col_piece, up_rows, preferred_element_type=jnp.float32)
    hidden = (jax.nn.silu(gate_part) * up_part).astype(jnp.bfloat16)
    partial_value = jnp.dot(hidden, w_down[0], preferred_element_type=jnp.float32)
    partial_value = partial_value.reshape(source_count, item_count, -1)
    summed = lax.psum_scatter(
        partial_value.astype(jnp.bfloat16), "tp", scatter_dimension=2, tiled=True
    )
    came_back = lax.all_to_all(summed, "ep", split_axis=0, concat_axis=0, tiled=True)
    picked = came_back.reshape(expert_count * capacity, -1)[dest_index].astype(jnp.float32)
    weighted = picked * gate_weights.reshape(-1)[:, None]
    return jnp.sum(weighted.reshape(tok_count, top_count, -1), axis=1).astype(jnp.bfloat16)


def solution(mesh):
    return jax.shard_map(
        fused if mesh.shape["tp"] == 4 else on_device,
        mesh=mesh,
        in_specs=(
            P(("grp", "ep"), "tp"),
            P(),
            P(("grp", "ep"), None),
            P(("grp", "ep"), None),
            P("ep", None, "tp"),
            P("ep", None, "tp"),
            P("ep", "tp", None),
        ),
        out_specs=P(("grp", "ep"), "tp"),
        check_vma=False,
    )
```

profile of v0, /device:TPU:0, one launch (start us, length us, event | category | flops | bytes accessed | tf_op | source)
XLA Modules:
  0.0 60.1 jit_solution(11467407843348987809)
XLA Ops:
  0.0 58.4 %shard_map.73 = bf16[256,512]{1,0:T(8,128)(2,1)} custom-call(bf16[256,512]{1,0:T(8,128)(2,1)} %tok_ref.1, s32[2,256]{1,0:T(2,128)} %bitcast.4, f32[2,256]{1,0:T(2,128)} %bitcast.5, f32[1,2048]{1,0:T(1,128)} %bitcast.3, bf16[1,2048,768]{2,1,0:T(8,128)(2,1)} %wg_ref.1, bf16[1,2048,768]{2,1,0:T(8,128)(2,1)} %wu_ref.1, bf16[1,768,2048]{2,1,0:T(8,128)(2,1)} %wd_ref.1), custom_call_target="tpu_custom_call" | custom-call | tf_op jit(solution)/shard_map/pallas_call | solution.py:354
  58.4 1.7 %copy.9 = bf16[256,512]{1,0:T(8,128)(2,1)} copy(bf16[256,512]{1,0:T(8,128)(2,1)} %shard_map.73) | data formatting | bytes 524288
where the time goes:
time: 60.2 us; the launch traced here: 60.1 us
  Pallas kernels  58.4 us (97%)
  local copies, waits for them, and re-layouts  1.67 us (3%)
    pallas_call x1, Pallas kernels, fused(): pl.pallas_call(functools.partial(layer_kernel, n_ep, cap, cuts), out_shap...  58.4 us
    unnamed x1, local copies, waits for them, and re-layouts  1.67 us

commit v1 on v0

--- a/solution.py
+++ b/solution.py
@@ -21,11 +21,48 @@
     return table
 
 
-def look_up(table, row, column):
-    value = jnp.int32(0)
-    for r, entries in enumerate(table):
-        for c, entry in enumerate(entries):
-            value = jnp.where((row == r) & (column == c), entry, value)
+def mirrored(units, count):
+    return [(count - 1 - s, h) for s, h in units]
+
+
+def unit_order(n_ep, cuts):
+    if (n_ep, cuts) == (4, 2):
+        outer = [(0, 0), (1, 0), (1, 1), (2, 0), (3, 1), (3, 0), (2, 1), (0, 1)]
+        inner = [(1, 0), (3, 0), (0, 1), (2, 0), (3, 1), (2, 1), (0, 0), (1, 1)]
+        both = [outer, inner, mirrored(inner, 4), mirrored(outer, 4)]
+    else:
+        both = [
+            [(s, h) for s in row for h in range(cuts)] for row in nearest_first(n_ep)
+        ]
+    return [[s * cuts + h for s, h in row] for row in both]
+
+
+def send_order(n_ep, cuts):
+    if (n_ep, cuts) == (4, 2):
+        outer = [(2, 0), (1, 1), (2, 1), (1, 0), (3, 1), (3, 0)]
+        inner = [(2, 0), (0, 0), (3, 0), (0, 1), (3, 1), (2, 1)]
+        both = [outer, inner, mirrored(inner, 4), mirrored(outer, 4)]
+    else:
+        both = [
+            [(s, h) for s in row[1:] for h in range(cuts)] for row in nearest_first(n_ep)
+        ]
+    return [[s * cuts + h for s, h in row] for row in both]
+
+
+def pick_row(table, row):
+    picked = []
+    for column in range(len(table[0])):
+        value = jnp.int32(table[0][column])
+        for r in range(1, len(table)):
+            value = jnp.where(row == r, table[r][column], value)
+        picked.append(value)
+    return picked
+
+
+def entry_of(entries, index):
+    value = entries[0]
+    for c in range(1, len(entries)):
+        value = jnp.where(index == c, entries[c], value)
     return value
 
 
@@ -82,7 +119,9 @@
     across = (tp + 2) % n_tp
     side = tp // 2
     table = nearest_first(n_ep)
-    order = [look_up(table, ep, i) for i in range(n_ep)]
+    order = pick_row(table, ep)
+    units = pick_row(unit_order(n_ep, cuts), ep)
+    sends = pick_row(send_order(n_ep, cuts), ep)
 
     weights = [
         pltpu.make_async_copy(wg_ref.at[0], wg, w_sem.at[0]),
@@ -212,27 +251,33 @@
 
     piece_rows = cap // cuts
     stages = n_ep * cuts
-    values = pack(1)
-    for h in range(cuts):
-        packed[order[1] * cuts + h] = values[h * piece_rows : (h + 1) * piece_rows]
+    for i in range(1, n_ep):
+        values = pack(i)
+        for h in range(cuts):
+            packed[order[i] * cuts + h] = values[h * piece_rows : (h + 1) * piece_rows]
     values = pack(0)
     for h in range(cuts):
         rows[ep * cuts + h, tp] = values[h * piece_rows : (h + 1) * piece_rows]
+
+    def unit_of(i):
+        return units[i] if isinstance(i, int) else entry_of(units, i)
+
+    def forward(i):
+        s = unit_of(i)
+
+        @pl.when(s // cuts != ep)
+        def _():
+            z_copy(s // cuts, s // cuts, s % cuts).wait_recv()
+
+        x_copy(s).start()
+        d_copy(s).start()
+
     pl.semaphore_wait(barrier, n_ep + 1)
-    for h in range(cuts):
-        z_copy(ep, order[1], h).start()
-        x_copy(ep * cuts + h).start()
-        d_copy(ep * cuts + h).start()
-    for i in range(2, n_ep):
-        values = pack(i)
-        for h in range(cuts):
-            packed[order[i] * cuts + h] = values[h * piece_rows : (h + 1) * piece_rows]
-            z_copy(ep, order[i], h).start()
+    for unit in sends:
+        z_copy(ep, unit // cuts, unit % cuts).start()
+    forward(0)
     for copy in weights:
         copy.wait()
-
-    def unit_of(i):
-        return look_up(table, ep, i // cuts) * cuts + i % cuts
 
     def finish(i):
         s = unit_of(i)
@@ -242,17 +287,11 @@
         total = total + from_chip[s].astype(jnp.float32)
         result[s] = total.astype(jnp.bfloat16)
 
-        @pl.when(i >= cuts)
+        @pl.when(s // cuts != ep)
         def _():
             r_copy(ep, s // cuts, s % cuts).start()
 
-    def forward(i):
-        s = unit_of(i)
-        z_copy(s // cuts, s // cuts, s % cuts).wait_recv()
-        x_copy(s).start()
-        d_copy(s).start()
-
-    for i in range(cuts, AHEAD):
+    for i in range(1, AHEAD):
         forward(i)
     x_copy(unit_of(0)).wait_recv()
     e_copy(unit_of(0)).start()
@@ -273,7 +312,7 @@
         gate_part = jnp.dot(normed[...], wg[...], preferred_element_type=jnp.float32)
         up_part = jnp.dot(normed[...], wu[...], preferred_element_type=jnp.float32)
         hidden[...] = (gate_part / (1.0 + jnp.exp(-gate_part)) * up_part).astype(jnp.bfloat16)
-        @pl.when((i + AHEAD >= cuts) & (i + AHEAD < stages))
+        @pl.when(i + AHEAD < stages)
         def _():
             forward(i + AHEAD)
 

time: 60.2 us -> 55.5 us (0.922)
  Pallas kernels: 58.4 us -> 53.6 us
    pallas_call x1, Pallas kernels: 58.4 us -> 53.6 us  [fused(): pl.pallas_call(functools.partial(layer_kernel, n_ep, cap, cuts), out_shap...]
where the time goes in v1:
time: 55.5 us; the launch traced here: 55.3 us
  Pallas kernels  53.6 us (97%)
  local copies, waits for them, and re-layouts  1.67 us (3%)
    pallas_call x1, Pallas kernels, fused(): pl.pallas_call(functools.partial(layer_kernel, n_ep, cap, cuts), out_shap...  53.6 us
    unnamed x1, local copies, waits for them, and re-layouts  1.67 us

profile of v1, /device:TPU:0, one launch (start us, length us, event | category | flops | bytes accessed | tf_op | source)
XLA Modules:
  0.0 55.3 jit_solution(932945195677847428)
XLA Ops:
  0.0 53.6 %shard_map.73 = bf16[256,512]{1,0:T(8,128)(2,1)} custom-call(bf16[256,512]{1,0:T(8,128)(2,1)} %tok_ref.1, s32[2,256]{1,0:T(2,128)} %bitcast.4, f32[2,256]{1,0:T(2,128)} %bitcast.5, f32[1,2048]{1,0:T(1,128)} %bitcast.3, bf16[1,2048,768]{2,1,0:T(8,128)(2,1)} %wg_ref.1, bf16[1,2048,768]{2,1,0:T(8,128)(2,1)} %wu_ref.1, bf16[1,768,2048]{2,1,0:T(8,128)(2,1)} %wd_ref.1), custom_call_target="tpu_custom_call" | custom-call | tf_op jit(solution)/shard_map/pallas_call | solution.py:393
  53.7 1.7 %copy.9 = bf16[256,512]{1,0:T(8,128)(2,1)} copy(bf16[256,512]{1,0:T(8,128)(2,1)} %shard_map.73) | data formatting | bytes 524288

commit v2 on v1

--- a/solution.py
+++ b/solution.py
@@ -27,20 +27,23 @@
 
 def unit_order(n_ep, cuts):
     if (n_ep, cuts) == (4, 2):
-        outer = [(0, 0), (1, 0), (1, 1), (2, 0), (3, 1), (3, 0), (2, 1), (0, 1)]
-        inner = [(1, 0), (3, 0), (0, 1), (2, 0), (3, 1), (2, 1), (0, 0), (1, 1)]
+        outer = [(0, 1), (1, 0), (2, 1), (3, 0), (3, 1), (2, 0), (1, 1), (0, 0)]
+        inner = [(1, 1), (3, 0), (0, 1), (2, 0), (3, 1), (0, 0), (2, 1), (1, 0)]
         both = [outer, inner, mirrored(inner, 4), mirrored(outer, 4)]
     else:
         both = [
-            [(s, h) for s in row for h in range(cuts)] for row in nearest_first(n_ep)
+            [(row[0], h) for h in range(cuts - 1)]
+            + [(s, h) for s in row[1:] for h in range(cuts)]
+            + [(row[0], cuts - 1)]
+            for row in nearest_first(n_ep)
         ]
     return [[s * cuts + h for s, h in row] for row in both]
 
 
 def send_order(n_ep, cuts):
     if (n_ep, cuts) == (4, 2):
-        outer = [(2, 0), (1, 1), (2, 1), (1, 0), (3, 1), (3, 0)]
-        inner = [(2, 0), (0, 0), (3, 0), (0, 1), (3, 1), (2, 1)]
+        outer = [(2, 0), (1, 1), (1, 0), (3, 0), (2, 1), (3, 1)]
+        inner = [(0, 0), (3, 1), (2, 0), (2, 1), (3, 0), (0, 1)]
         both = [outer, inner, mirrored(inner, 4), mirrored(outer, 4)]
     else:
         both = [
@@ -70,20 +73,24 @@
     n_ep,
     cap,
     cuts,
+    tok_hbm,
+    ids_hbm,
+    gate_hbm,
+    gain_hbm,
+    wg_ref,
+    wu_ref,
+    wd_ref,
+    out_ref,
     tok_ref,
     ids_ref,
     gate_ref,
     gain_ref,
-    wg_ref,
-    wu_ref,
-    wd_ref,
-    out_ref,
+    acc,
     wg,
     wu,
     wd,
     packed,
     rows,
-    normed,
     hidden,
     own,
     to_core,
@@ -93,6 +100,7 @@
     result,
     back,
     w_sem,
+    i_sem,
     z_send,
     z_recv,
     x_send,
@@ -111,6 +119,7 @@
     tok_count, col_count = tok_ref.shape
     top_count = ids_ref.shape[0]
     n_tp = rows.shape[1]
+    units = wg.shape[1]
     width = n_tp * col_count
     ep = lax.axis_index("ep")
     tp = lax.axis_index("tp")
@@ -118,9 +127,31 @@
     sibling = tp + 1 - 2 * core
     across = (tp + 2) % n_tp
     side = tp // 2
+    barrier = pltpu.get_barrier_semaphore()
+    for step in range(1, n_ep):
+        pl.semaphore_signal(
+            barrier, inc=1, device_id={"ep": (ep + step) % n_ep}, device_id_type=MESH
+        )
+    for peer in (sibling, across):
+        pl.semaphore_signal(barrier, inc=1, device_id={"tp": peer}, device_id_type=MESH)
+
+    inputs = [
+        pltpu.make_async_copy(source, target, i_sem.at[n])
+        for n, (source, target) in enumerate(
+            [
+                (ids_hbm, ids_ref),
+                (gate_hbm, gate_ref),
+                (tok_hbm, tok_ref),
+                (gain_hbm, gain_ref),
+            ]
+        )
+    ]
+    for copy in inputs:
+        copy.start()
+
     table = nearest_first(n_ep)
     order = pick_row(table, ep)
-    units = pick_row(unit_order(n_ep, cuts), ep)
+    turns = pick_row(unit_order(n_ep, cuts), ep)
     sends = pick_row(send_order(n_ep, cuts), ep)
 
     weights = [
@@ -138,17 +169,8 @@
         weights.append(
             pltpu.make_async_copy(wd_ref.at[0, :, cols], wd.at[j], w_sem.at[2 + j])
         )
-    for copy in weights:
-        copy.start()
-
-    barrier = pltpu.get_barrier_semaphore()
-    for step in range(1, n_ep):
-        pl.semaphore_signal(
-            barrier, inc=1, device_id={"ep": (ep + step) % n_ep}, device_id_type=MESH
-        )
-    for peer in (sibling, across):
-        pl.semaphore_signal(barrier, inc=1, device_id={"tp": peer}, device_id_type=MESH)
-
+    inputs[0].wait()
+    inputs[1].wait()
     lane = lax.broadcasted_iota(jnp.int32, (tok_count, 128), 1)
     lane_expert = jnp.full((tok_count, 128), -1, jnp.int32)
     for i in range(n_ep):
@@ -183,7 +205,7 @@
         return pltpu.make_async_remote_copy(
             src_ref=packed.at[there * cuts + h],
             dst_ref=rows.at[here * cuts + h, tp],
-            send_sem=z_send.at[there * cuts + h],
+            send_sem=z_send,
             recv_sem=z_recv.at[here * cuts + h],
             device_id={"ep": there},
             device_id_type=MESH,
@@ -193,7 +215,7 @@
         return pltpu.make_async_remote_copy(
             src_ref=rows.at[i, tp],
             dst_ref=rows.at[i, tp],
-            send_sem=x_send.at[i],
+            send_sem=x_send,
             recv_sem=x_recv.at[i],
             device_id={"tp": across},
             device_id_type=MESH,
@@ -203,7 +225,7 @@
         return pltpu.make_async_remote_copy(
             src_ref=rows.at[i, tp],
             dst_ref=rows.at[i, tp],
-            send_sem=d_send.at[i],
+            send_sem=d_send,
             recv_sem=d_recv.at[i],
             device_id={"tp": sibling},
             device_id_type=MESH,
@@ -213,7 +235,7 @@
         return pltpu.make_async_remote_copy(
             src_ref=rows.at[i, across],
             dst_ref=rows.at[i, across],
-            send_sem=e_send.at[i],
+            send_sem=e_send,
             recv_sem=e_recv.at[i],
             device_id={"tp": sibling},
             device_id_type=MESH,
@@ -223,7 +245,7 @@
         return pltpu.make_async_remote_copy(
             src_ref=to_core.at[i, j],
             dst_ref=from_core.at[i, j],
-            send_sem=pc_send.at[i, j],
+            send_sem=pc_send,
             recv_sem=pc_recv.at[i, j],
             device_id={"tp": sibling},
             device_id_type=MESH,
@@ -233,7 +255,7 @@
         return pltpu.make_async_remote_copy(
             src_ref=to_chip.at[i],
             dst_ref=from_chip.at[i],
-            send_sem=px_send.at[i],
+            send_sem=px_send,
             recv_sem=px_recv.at[i],
             device_id={"tp": across},
             device_id_type=MESH,
@@ -243,7 +265,7 @@
         return pltpu.make_async_remote_copy(
             src_ref=result.at[there * cuts + h],
             dst_ref=back.at[here * cuts + h],
-            send_sem=r_send.at[there * cuts + h],
+            send_sem=r_send,
             recv_sem=r_recv.at[here * cuts + h],
             device_id={"ep": there},
             device_id_type=MESH,
@@ -251,6 +273,9 @@
 
     piece_rows = cap // cuts
     stages = n_ep * cuts
+    inputs[2].wait()
+    for copy in weights:
+        copy.start()
     for i in range(1, n_ep):
         values = pack(i)
         for h in range(cuts):
@@ -260,7 +285,11 @@
         rows[ep * cuts + h, tp] = values[h * piece_rows : (h + 1) * piece_rows]
 
     def unit_of(i):
-        return units[i] if isinstance(i, int) else entry_of(units, i)
+        return turns[i] if isinstance(i, int) else entry_of(turns, i)
+
+    def spread(s):
+        x_copy(s).start()
+        d_copy(s).start()
 
     def forward(i):
         s = unit_of(i)
@@ -268,16 +297,29 @@
         @pl.when(s // cuts != ep)
         def _():
             z_copy(s // cuts, s // cuts, s % cuts).wait_recv()
-
-        x_copy(s).start()
-        d_copy(s).start()
+            spread(s)
 
     pl.semaphore_wait(barrier, n_ep + 1)
     for unit in sends:
         z_copy(ep, unit // cuts, unit % cuts).start()
-    forward(0)
+    for h in range(cuts):
+        spread(ep * cuts + h)
+    inputs[3].wait()
     for copy in weights:
         copy.wait()
+
+    def scale(i, carry):
+        block = pl.ds(pl.multiple_of(i * 128, 128), 128)
+        gain = jnp.broadcast_to(gain_ref[:, block], (128, 128)).T
+        for matrix in (wg, wu):
+            for c in range(units // 128):
+                cols = slice(c * 128, (c + 1) * 128)
+                matrix[block, cols] = (matrix[block, cols].astype(jnp.float32) * gain).astype(
+                    jnp.bfloat16
+                )
+        return carry
+
+    lax.fori_loop(0, width // 128, scale, 0)
 
     def finish(i):
         s = unit_of(i)
@@ -305,13 +347,25 @@
             part = rows[s, k].astype(jnp.float32)
             square_sum = square_sum + jnp.sum(part * part, axis=1, keepdims=True)
         factor = lax.rsqrt(square_sum / width + epsilon)
-        for k in range(n_tp):
-            cols = slice(k * col_count, (k + 1) * col_count)
-            part = rows[s, k].astype(jnp.float32)
-            normed[:, cols] = (part * factor * gain_ref[:, cols]).astype(jnp.bfloat16)
-        gate_part = jnp.dot(normed[...], wg[...], preferred_element_type=jnp.float32)
-        up_part = jnp.dot(normed[...], wu[...], preferred_element_type=jnp.float32)
-        hidden[...] = (gate_part / (1.0 + jnp.exp(-gate_part)) * up_part).astype(jnp.bfloat16)
+        for c in range(units // 256):
+            cols = slice(c * 256, (c + 1) * 256)
+            gate_part = jnp.zeros((piece_rows, 256), jnp.float32)
+            up_part = jnp.zeros((piece_rows, 256), jnp.float32)
+            for k in range(n_tp):
+                depth = slice(k * col_count, (k + 1) * col_count)
+                part = rows[s, k]
+                gate_part = gate_part + jnp.dot(
+                    part, wg[depth, cols], preferred_element_type=jnp.float32
+                )
+                up_part = up_part + jnp.dot(
+                    part, wu[depth, cols], preferred_element_type=jnp.float32
+                )
+            gate_part = gate_part * factor
+            up_part = up_part * factor
+            hidden[:, cols] = (gate_part / (1.0 + jnp.exp(-gate_part)) * up_part).astype(
+                jnp.bfloat16
+            )
+
         @pl.when(i + AHEAD < stages)
         def _():
             forward(i + AHEAD)
@@ -340,40 +394,50 @@
         return carry
 
     lax.fori_loop(0, stages, stage, 0)
-    for i in range(stages - LAG, stages):
+    for i in range(stages - LAG, stages - 1):
         finish(i)
 
     slot_lanes = lax.broadcasted_iota(jnp.int32, (tok_count, piece_rows), 1).astype(
         jnp.float32
     )
+
+    def unpack(i, h, values):
+        pick = jnp.where(slot_lanes + h * piece_rows == place[:, i : i + 1], 1.0, 0.0)
+        return jnp.dot(pick.astype(jnp.bfloat16), values, preferred_element_type=jnp.float32)
+
     mixed = jnp.zeros((tok_count, col_count), jnp.float32)
-    for i in range(n_ep):
+    for i in range(1, n_ep):
         taken = jnp.zeros((tok_count, col_count), jnp.float32)
         for h in range(cuts):
-            pick = jnp.where(slot_lanes + h * piece_rows == place[:, i : i + 1], 1.0, 0.0)
-            unit = order[i] * cuts + h
-            if i == 0:
-                values = result[unit]
-            else:
-                r_copy(order[i], order[i], h).wait_recv()
-                values = back[unit]
-            taken = taken + jnp.dot(
-                pick.astype(jnp.bfloat16), values, preferred_element_type=jnp.float32
-            )
+            r_copy(order[i], order[i], h).wait_recv()
+            taken = taken + unpack(i, h, back[order[i] * cuts + h])
         mixed = mixed + weight[:, i : i + 1] * taken
-    out_ref[...] = mixed.astype(jnp.bfloat16)
-
-    for i in range(1, n_ep):
-        for h in range(cuts):
-            z_copy(ep, order[i], h).wait_send()
-            r_copy(ep, order[i], h).wait_send()
-    for i in range(stages):
-        x_copy(i).wait_send()
-        d_copy(i).wait_send()
-        e_copy(i).wait_send()
-        pc_copy(i, 0).wait_send()
-        pc_copy(i, 1).wait_send()
-        px_copy(i).wait_send()
+    acc[...] = mixed
+
+    def drain(pieces, sem):
+        pltpu.make_async_remote_copy(
+            src_ref=pieces,
+            dst_ref=pieces,
+            send_sem=sem,
+            recv_sem=px_recv.at[0],
+            device_id={"tp": across},
+            device_id_type=MESH,
+        ).wait_send()
+
+    others = stages - cuts
+    drain(packed.at[pl.ds(0, others)], z_send)
+    drain(result.at[pl.ds(0, others)], r_send)
+    drain(to_chip, x_send)
+    drain(to_chip, d_send)
+    drain(to_chip, e_send)
+    drain(to_core, pc_send)
+
+    finish(stages - 1)
+    taken = jnp.zeros((tok_count, col_count), jnp.float32)
+    for h in range(cuts):
+        taken = taken + unpack(0, h, result[ep * cuts + h])
+    out_ref[...] = (acc[...] + weight[:, 0:1] * taken).astype(jnp.bfloat16)
+    drain(to_chip, px_send)
 
 
 def fused(tokens, norm_gain, expert_ids, gate_weights, w_gate, w_up, w_down):
@@ -393,25 +457,29 @@
     return pl.pallas_call(
         functools.partial(layer_kernel, n_ep, cap, cuts),
         out_shape=jax.ShapeDtypeStruct((tok_count, col_count), bf16),
-        in_specs=[vmem] * 4 + [anywhere] * 3,
+        in_specs=[anywhere] * 7,
         out_specs=vmem,
         scratch_shapes=[
+            pltpu.VMEM((tok_count, col_count), bf16),
+            pltpu.VMEM((top_count, tok_count), jnp.int32),
+            pltpu.VMEM((top_count, tok_count), jnp.float32),
+            pltpu.VMEM((1, width), jnp.float32),
+            pltpu.VMEM((tok_count, col_count), jnp.float32),
             pltpu.VMEM((width, units), bf16),
             pltpu.VMEM((width, units), bf16),
             pltpu.VMEM((n_tp, units, col_count), bf16),
             pltpu.VMEM((stages, piece_rows, col_count), bf16),
             pltpu.VMEM((stages, n_tp, piece_rows, col_count), bf16),
-            pltpu.VMEM((piece_rows, width), bf16),
             pltpu.VMEM((piece_rows, units), bf16),
             pltpu.VMEM((LAG + 1, piece_rows, col_count), jnp.float32),
             pltpu.VMEM((stages, 2, piece_rows, col_count), bf16),
             pltpu.VMEM((stages, 2, piece_rows, col_count), bf16),
         ]
         + [pltpu.VMEM((stages, piece_rows, col_count), bf16)] * 4
-        + [sems((2 + n_tp,))]
-        + [sems((stages,))] * 8
-        + [sems((stages, 2))] * 2
-        + [sems((stages,))] * 4,
+        + [sems((2 + n_tp,)), sems((4,))]
+        + [sems, sems((stages,))] * 4
+        + [sems, sems((stages, 2))]
+        + [sems, sems((stages,))] * 2,
         compiler_params=pltpu.CompilerParams(
             collective_id=0, has_side_effects=True, vmem_limit_bytes=56 * 2**20
         ),

time: 55.5 us -> 50.5 us (0.910)
  Pallas kernels: 53.6 us -> 48.7 us
    pallas_call x1, Pallas kernels: 53.6 us -> 48.7 us  [fused(): pl.pallas_call(functools.partial(layer_kernel, n_ep, cap, cuts), out_shap...]
where the time goes in v2:
time: 50.5 us; the launch traced here: 50.4 us
  Pallas kernels  48.7 us (96%)
  local copies, waits for them, and re-layouts  1.67 us (3%)
    pallas_call x1, Pallas kernels, fused(): pl.pallas_call(functools.partial(layer_kernel, n_ep, cap, cuts), out_shap...  48.7 us
    unnamed x1, local copies, waits for them, and re-layouts  1.67 us

profile of v2, /device:TPU:0, one launch (start us, length us, event | category | flops | bytes accessed | tf_op | source)
XLA Modules:
  0.0 50.4 jit_solution(9095184047904524459)
XLA Ops:
  0.0 48.7 %shard_map.73 = bf16[256,512]{1,0:T(8,128)(2,1)} custom-call(bf16[256,512]{1,0:T(8,128)(2,1)} %tok_hbm.1, s32[2,256]{1,0:T(2,128)} %bitcast.4, f32[2,256]{1,0:T(2,128)} %bitcast.5, f32[1,2048]{1,0:T(1,128)} %bitcast.3, bf16[1,2048,768]{2,1,0:T(8,128)(2,1)} %wg_ref.1, bf16[1,2048,768]{2,1,0:T(8,128)(2,1)} %wu_ref.1, bf16[1,768,2048]{2,1,0:T(8,128)(2,1)} %wd_ref.1), custom_call_target="tpu_custom_call" | custom-call | tf_op jit(solution)/shard_map/pallas_call | solution.py:457
  48.7 1.7 %copy.9 = bf16[256,512]{1,0:T(8,128)(2,1)} copy(bf16[256,512]{1,0:T(8,128)(2,1)} %shard_map.73) | data formatting | bytes 524288

commit v3 on v2

--- a/solution.py
+++ b/solution.py
@@ -9,7 +9,7 @@
 
 epsilon = 1e-06
 AHEAD = 2
-LAG = 1
+LAG = 2
 MESH = pl.DeviceIdType.MESH
 
 
@@ -50,6 +50,10 @@
             [(s, h) for s in row[1:] for h in range(cuts)] for row in nearest_first(n_ep)
         ]
     return [[s * cuts + h for s, h in row] for row in both]
+
+
+def first_named(units, cuts):
+    return list(dict.fromkeys(unit // cuts for unit in units))
 
 
 def pick_row(table, row):
@@ -149,8 +153,7 @@
     for copy in inputs:
         copy.start()
 
-    table = nearest_first(n_ep)
-    order = pick_row(table, ep)
+    order = [ep] + pick_row([first_named(row, cuts) for row in send_order(n_ep, cuts)], ep)
     turns = pick_row(unit_order(n_ep, cuts), ep)
     sends = pick_row(send_order(n_ep, cuts), ep)
 
@@ -274,39 +277,41 @@
     piece_rows = cap // cuts
     stages = n_ep * cuts
     inputs[2].wait()
-    for copy in weights:
+    for copy in weights[:2]:
         copy.start()
+    values = pack(0)
+    for h in range(cuts):
+        rows[ep * cuts + h, tp] = values[h * piece_rows : (h + 1) * piece_rows]
+
+    def unit_of(i):
+        return turns[i] if isinstance(i, int) else entry_of(turns, i)
+
+    def spread(s):
+        x_copy(s).start()
+        d_copy(s).start()
+
+    def forward(i):
+        s = unit_of(i)
+
+        @pl.when(s // cuts != ep)
+        def _():
+            z_copy(s // cuts, s // cuts, s % cuts).wait_recv()
+            spread(s)
+
+    pl.semaphore_wait(barrier, n_ep + 1)
+    for h in range(cuts):
+        spread(ep * cuts + h)
     for i in range(1, n_ep):
         values = pack(i)
         for h in range(cuts):
             packed[order[i] * cuts + h] = values[h * piece_rows : (h + 1) * piece_rows]
-    values = pack(0)
-    for h in range(cuts):
-        rows[ep * cuts + h, tp] = values[h * piece_rows : (h + 1) * piece_rows]
-
-    def unit_of(i):
-        return turns[i] if isinstance(i, int) else entry_of(turns, i)
-
-    def spread(s):
-        x_copy(s).start()
-        d_copy(s).start()
-
-    def forward(i):
-        s = unit_of(i)
-
-        @pl.when(s // cuts != ep)
-        def _():
-            z_copy(s // cuts, s // cuts, s % cuts).wait_recv()
-            spread(s)
-
-    pl.semaphore_wait(barrier, n_ep + 1)
-    for unit in sends:
-        z_copy(ep, unit // cuts, unit % cuts).start()
-    for h in range(cuts):
-        spread(ep * cuts + h)
+        for unit in sends[i - 1 :] if i + 1 == n_ep else sends[i - 1 : i]:
+            z_copy(ep, unit // cuts, unit % cuts).start()
     inputs[3].wait()
-    for copy in weights:
+    for copy in weights[:2]:
         copy.wait()
+    for copy in weights[2:]:
+        copy.start()
 
     def scale(i, carry):
         block = pl.ds(pl.multiple_of(i * 128, 128), 128)
@@ -319,7 +324,7 @@
                 )
         return carry
 
-    lax.fori_loop(0, width // 128, scale, 0)
+    lax.fori_loop(0, width // 128, scale, 0, unroll=2)
 
     def finish(i):
         s = unit_of(i)
@@ -337,6 +342,8 @@
         forward(i)
     x_copy(unit_of(0)).wait_recv()
     e_copy(unit_of(0)).start()
+    for copy in weights[2:]:
+        copy.wait()
 
     def stage(i, carry):
         s = unit_of(i)
@@ -366,30 +373,33 @@
                 jnp.bfloat16
             )
 
+        @pl.when(i >= LAG)
+        def _():
+            finish(i - LAG)
+
         @pl.when(i + AHEAD < stages)
         def _():
             forward(i + AHEAD)
+
+        to_core[s, 0] = jnp.dot(
+            hidden[...], wd[0], preferred_element_type=jnp.float32
+        ).astype(jnp.bfloat16)
+        pc_copy(s, 0).start()
+        to_core[s, 1] = jnp.dot(
+            hidden[...], wd[1], preferred_element_type=jnp.float32
+        ).astype(jnp.bfloat16)
+        part = jnp.dot(hidden[...], wd[2], preferred_element_type=jnp.float32)
+        own[i % (LAG + 1)] = jnp.dot(hidden[...], wd[3], preferred_element_type=jnp.float32)
+        pc_copy(s, 1).start()
+        pc_copy(s, 0).wait_recv()
+        to_chip[s] = (part + from_core[s, 0].astype(jnp.float32)).astype(jnp.bfloat16)
+        px_copy(s).start()
 
         @pl.when(i + 1 < stages)
         def _():
             after = unit_of(i + 1)
             x_copy(after).wait_recv()
             e_copy(after).start()
-
-        for j in range(2):
-            to_core[s, j] = jnp.dot(
-                hidden[...], wd[j], preferred_element_type=jnp.float32
-            ).astype(jnp.bfloat16)
-            pc_copy(s, j).start()
-        part = jnp.dot(hidden[...], wd[2], preferred_element_type=jnp.float32)
-        own[i % (LAG + 1)] = jnp.dot(hidden[...], wd[3], preferred_element_type=jnp.float32)
-        pc_copy(s, 0).wait_recv()
-        to_chip[s] = (part + from_core[s, 0].astype(jnp.float32)).astype(jnp.bfloat16)
-        px_copy(s).start()
-
-        @pl.when(i >= LAG)
-        def _():
-            finish(i - LAG)
 
         return carry
 
@@ -481,16 +491,21 @@
         + [sems, sems((stages, 2))]
         + [sems, sems((stages,))] * 2,
         compiler_params=pltpu.CompilerParams(
-            collective_id=0, has_side_effects=True, vmem_limit_bytes=56 * 2**20
+            collective_id=0, has_side_effects=True, vmem_limit_bytes=40 * 2**20
         ),
     )(
-        tokens,
-        expert_ids.T,
-        gate_weights.T,
-        norm_gain.reshape(1, width),
-        w_gate,
-        w_up,
-        w_down,
+        *(
+            pltpu.with_memory_space_constraint(operand, pltpu.HBM)
+            for operand in (
+                tokens,
+                expert_ids.T,
+                gate_weights.T,
+                norm_gain.reshape(1, width),
+                w_gate,
+                w_up,
+                w_down,
+            )
+        )
     )
 
 

time: 50.5 us -> 48.3 us (0.956)
  Pallas kernels: 48.7 us -> 47.4 us
  local copies, waits for them, and re-layouts: 1.67 us -> 0.71 us
    pallas_call x1, Pallas kernels: 48.7 us -> 47.4 us  [fused(): pl.pallas_call(functools.partial(layer_kernel, n_ep, cap, cuts), out_shap...]
    unnamed x1, local copies, waits for them, and re-layouts: 1.67 us -> 0.71 us
where the time goes in v3:
time: 48.3 us; the launch traced here: 48.1 us
  Pallas kernels  47.4 us (98%)
  local copies, waits for them, and re-layouts  0.71 us (1%)
    pallas_call x1, Pallas kernels, fused(): pl.pallas_call(functools.partial(layer_kernel, n_ep, cap, cuts), out_shap...  47.4 us

profile of v3, /device:TPU:0, one launch (start us, length us, event | category | flops | bytes accessed | tf_op | source)
XLA Modules:
  0.0 48.1 jit_solution(15184705584145036112)
XLA Ops:
  0.0 47.4 %shard_map.73 = bf16[256,512]{1,0:T(8,128)(2,1)S(1)} custom-call(bf16[256,512]{1,0:T(8,128)(2,1)} %tok_hbm.1, s32[2,256]{1,0:T(2,128)} %bitcast.4, f32[2,256]{1,0:T(2,128)} %bitcast.5, f32[1,2048]{1,0:T(1,128)} %bitcast.3, bf16[1,2048,768]{2,1,0:T(8,128)(2,1)} %wg_ref.1, bf16[1,2048,768]{2,1,0:T(8,128)(2,1)} %wu_ref.1, bf16[1,768,2048]{2,1,0:T(8,128)(2,1)} %wd_ref.1), custom_call_target="tpu_custom_call" | custom-call | tf_op jit(solution)/shard_map/pallas_call | solution.py:467
  47.4 0.7 %copy.9 = bf16[256,512]{1,0:T(8,128)(2,1)} copy(bf16[256,512]{1,0:T(8,128)(2,1)S(1)} %shard_map.73) | data formatting | bytes 524288

commit v4 on v3

--- a/solution.py
+++ b/solution.py
@@ -21,35 +21,37 @@
     return table
 
 
-def mirrored(units, count):
-    return [(count - 1 - s, h) for s, h in units]
-
-
 def unit_order(n_ep, cuts):
     if (n_ep, cuts) == (4, 2):
-        outer = [(0, 1), (1, 0), (2, 1), (3, 0), (3, 1), (2, 0), (1, 1), (0, 0)]
-        inner = [(1, 1), (3, 0), (0, 1), (2, 0), (3, 1), (0, 0), (2, 1), (1, 0)]
-        both = [outer, inner, mirrored(inner, 4), mirrored(outer, 4)]
+        rows = [
+            [(0, 1), (1, 0), (2, 1), (3, 0), (3, 1), (2, 0), (1, 1), (0, 0)],
+            [(1, 1), (3, 0), (0, 1), (2, 0), (3, 1), (0, 0), (2, 1), (1, 0)],
+            [(2, 1), (3, 1), (0, 0), (0, 1), (1, 0), (1, 1), (3, 0), (2, 0)],
+            [(3, 1), (2, 0), (1, 1), (0, 0), (0, 1), (1, 0), (2, 1), (3, 0)],
+        ]
     else:
-        both = [
+        rows = [
             [(row[0], h) for h in range(cuts - 1)]
             + [(s, h) for s in row[1:] for h in range(cuts)]
             + [(row[0], cuts - 1)]
             for row in nearest_first(n_ep)
         ]
-    return [[s * cuts + h for s, h in row] for row in both]
+    return [[s * cuts + h for s, h in row] for row in rows]
 
 
 def send_order(n_ep, cuts):
     if (n_ep, cuts) == (4, 2):
-        outer = [(2, 0), (1, 1), (1, 0), (3, 0), (2, 1), (3, 1)]
-        inner = [(0, 0), (3, 1), (2, 0), (2, 1), (3, 0), (0, 1)]
-        both = [outer, inner, mirrored(inner, 4), mirrored(outer, 4)]
+        rows = [
+            [(2, 0), (1, 1), (1, 0), (3, 0), (2, 1), (3, 1)],
+            [(0, 0), (3, 1), (2, 1), (3, 0), (2, 0), (0, 1)],
+            [(0, 1), (3, 0), (1, 0), (1, 1), (0, 0), (3, 1)],
+            [(1, 0), (2, 1), (2, 0), (0, 0), (1, 1), (0, 1)],
+        ]
     else:
-        both = [
+        rows = [
             [(s, h) for s in row[1:] for h in range(cuts)] for row in nearest_first(n_ep)
         ]
-    return [[s * cuts + h for s, h in row] for row in both]
+    return [[s * cuts + h for s, h in row] for row in rows]
 
 
 def first_named(units, cuts):
@@ -174,28 +176,25 @@
         )
     inputs[0].wait()
     inputs[1].wait()
-    lane = lax.broadcasted_iota(jnp.int32, (tok_count, 128), 1)
-    lane_expert = jnp.full((tok_count, 128), -1, jnp.int32)
+    columns = -(-n_ep // 16) * 16
+    column = lax.broadcasted_iota(jnp.int32, (columns, tok_count), 0)
+    column_expert = jnp.full((columns, tok_count), -1, jnp.int32)
     for i in range(n_ep):
-        lane_expert = jnp.where(lane == i, order[i], lane_expert)
-    ids = ids_ref[...].astype(jnp.float32).T
-    gates = gate_ref[...].T
-    lane_expert = lane_expert.astype(jnp.float32)
-    named = jnp.zeros((tok_count, 128), jnp.float32)
-    weight = jnp.zeros((tok_count, 128), jnp.float32)
+        column_expert = jnp.where(column == i, order[i], column_expert)
+    named = jnp.zeros((columns, tok_count), jnp.float32)
+    weight_t = jnp.zeros((columns, tok_count), jnp.float32)
     for k in range(top_count):
-        hit = ids[:, k : k + 1] == lane_expert
+        hit = ids_ref[k : k + 1, :] == column_expert
         named = named + jnp.where(hit, 1.0, 0.0)
-        weight = weight + jnp.where(hit, gates[:, k : k + 1], 0.0)
+        weight_t = weight_t + jnp.where(hit, gate_ref[k : k + 1, :], 0.0)
     before = jnp.where(
-        lax.broadcasted_iota(jnp.int32, (tok_count, tok_count), 1)
-        < lax.broadcasted_iota(jnp.int32, (tok_count, tok_count), 0),
+        lax.broadcasted_iota(jnp.int32, (tok_count, tok_count), 0)
+        < lax.broadcasted_iota(jnp.int32, (tok_count, tok_count), 1),
         1.0,
         0.0,
     ).astype(jnp.bfloat16)
-    place = jnp.dot(before, named.astype(jnp.bfloat16), preferred_element_type=jnp.float32)
-    place = jnp.where(named > 0.0, place, -1.0)
-    place_t = place.T
+    place_t = jnp.dot(named.astype(jnp.bfloat16), before, preferred_element_type=jnp.float32)
+    place_t = jnp.where(named > 0.0, place_t, -1.0)
     slot_rows = lax.broadcasted_iota(jnp.int32, (cap, tok_count), 0).astype(jnp.float32)
 
     def pack(i):
@@ -391,16 +390,22 @@
         part = jnp.dot(hidden[...], wd[2], preferred_element_type=jnp.float32)
         own[i % (LAG + 1)] = jnp.dot(hidden[...], wd[3], preferred_element_type=jnp.float32)
         pc_copy(s, 1).start()
-        pc_copy(s, 0).wait_recv()
-        to_chip[s] = (part + from_core[s, 0].astype(jnp.float32)).astype(jnp.bfloat16)
-        px_copy(s).start()
-
-        @pl.when(i + 1 < stages)
+
+        @pl.when(i + 2 < stages)
         def _():
             after = unit_of(i + 1)
             x_copy(after).wait_recv()
             e_copy(after).start()
 
+        @pl.when(i == 1)
+        def _():
+            x_copy(unit_of(stages - 1)).wait_recv()
+            e_copy(unit_of(stages - 1)).start()
+
+        pc_copy(s, 0).wait_recv()
+        to_chip[s] = (part + from_core[s, 0].astype(jnp.float32)).astype(jnp.bfloat16)
+        px_copy(s).start()
+
         return carry
 
     lax.fori_loop(0, stages, stage, 0)
@@ -411,8 +416,12 @@
         jnp.float32
     )
 
+    place = place_t.T
+    weight = weight_t.T
+
     def unpack(i, h, values):
-        pick = jnp.where(slot_lanes + h * piece_rows == place[:, i : i + 1], 1.0, 0.0)
+        start = jnp.asarray(h * piece_rows, jnp.int32).astype(jnp.float32)
+        pick = jnp.where(slot_lanes + start == place[:, i : i + 1], 1.0, 0.0)
         return jnp.dot(pick.astype(jnp.bfloat16), values, preferred_element_type=jnp.float32)
 
     mixed = jnp.zeros((tok_count, col_count), jnp.float32)
@@ -422,6 +431,10 @@
             r_copy(order[i], order[i], h).wait_recv()
             taken = taken + unpack(i, h, back[order[i] * cuts + h])
         mixed = mixed + weight[:, i : i + 1] * taken
+    last = turns[stages - 1] % cuts
+    for step in range(1, cuts):
+        h = (last + step) % cuts
+        mixed = mixed + weight[:, 0:1] * unpack(0, h, result[ep * cuts + h])
     acc[...] = mixed
 
     def drain(pieces, sem):
@@ -443,9 +456,7 @@
     drain(to_core, pc_send)
 
     finish(stages - 1)
-    taken = jnp.zeros((tok_count, col_count), jnp.float32)
-    for h in range(cuts):
-        taken = taken + unpack(0, h, result[ep * cuts + h])
+    taken = unpack(0, last, result[ep * cuts + last])
     out_ref[...] = (acc[...] + weight[:, 0:1] * taken).astype(jnp.bfloat16)
     drain(to_chip, px_send)
 

time: 48.3 us -> 47.6 us (0.986)
  Pallas kernels: 47.4 us -> 46.3 us
    pallas_call x1, Pallas kernels: 47.4 us -> 46.3 us  [fused(): pl.pallas_call(functools.partial(layer_kernel, n_ep, cap, cuts), out_shap...]
where the time goes in v4:
time: 47.6 us; the launch traced here: 47 us
  Pallas kernels  46.3 us (97%)
  local copies, waits for them, and re-layouts  0.71 us (1%)
    pallas_call x1, Pallas kernels, fused(): pl.pallas_call(functools.partial(layer_kernel, n_ep, cap, cuts), out_shap...  46.3 us

profile of v4, /device:TPU:0, one launch (start us, length us, event | category | flops | bytes accessed | tf_op | source)
XLA Modules:
  0.0 47.0 jit_solution(6963038037141251671)
XLA Ops:
  0.0 46.3 %shard_map.73 = bf16[256,512]{1,0:T(8,128)(2,1)S(1)} custom-call(bf16[256,512]{1,0:T(8,128)(2,1)} %tok_hbm.1, s32[2,256]{1,0:T(2,128)} %bitcast.4, f32[2,256]{1,0:T(2,128)} %bitcast.5, f32[1,2048]{1,0:T(1,128)} %bitcast.3, bf16[1,2048,768]{2,1,0:T(8,128)(2,1)} %wg_ref.1, bf16[1,2048,768]{2,1,0:T(8,128)(2,1)} %wu_ref.1, bf16[1,768,2048]{2,1,0:T(8,128)(2,1)} %wd_ref.1), custom_call_target="tpu_custom_call" | custom-call | tf_op jit(solution)/shard_map/pallas_call | solution.py:478
  46.3 0.7 %copy.9 = bf16[256,512]{1,0:T(8,128)(2,1)} copy(bf16[256,512]{1,0:T(8,128)(2,1)S(1)} %shard_map.73) | data formatting | bytes 524288

commit v5 on v4

--- a/solution.py
+++ b/solution.py
@@ -114,7 +114,6 @@
     d_send,
     d_recv,
     e_send,
-    e_recv,
     pc_send,
     pc_recv,
     px_send,
@@ -238,7 +237,7 @@
             src_ref=rows.at[i, across],
             dst_ref=rows.at[i, across],
             send_sem=e_send,
-            recv_sem=e_recv.at[i],
+            recv_sem=d_recv.at[i],
             device_id={"tp": sibling},
             device_id_type=MESH,
         )
@@ -298,8 +297,9 @@
             spread(s)
 
     pl.semaphore_wait(barrier, n_ep + 1)
-    for h in range(cuts):
-        spread(ep * cuts + h)
+    first = turns[0] % cuts
+    for step in range(cuts):
+        spread(ep * cuts + (first + step) % cuts)
     for i in range(1, n_ep):
         values = pack(i)
         for h in range(cuts):
@@ -346,8 +346,15 @@
 
     def stage(i, carry):
         s = unit_of(i)
-        d_copy(s).wait_recv()
-        e_copy(s).wait_recv()
+        pair = rows.at[s, pl.ds(0, 2)]
+        pltpu.make_async_remote_copy(
+            src_ref=pair,
+            dst_ref=pair,
+            send_sem=d_send,
+            recv_sem=d_recv.at[s],
+            device_id={"tp": sibling},
+            device_id_type=MESH,
+        ).wait_recv()
         square_sum = jnp.zeros((piece_rows, 1), jnp.float32)
         for k in range(n_tp):
             part = rows[s, k].astype(jnp.float32)
@@ -498,7 +505,8 @@
         ]
         + [pltpu.VMEM((stages, piece_rows, col_count), bf16)] * 4
         + [sems((2 + n_tp,)), sems((4,))]
-        + [sems, sems((stages,))] * 4
+        + [sems, sems((stages,))] * 3
+        + [sems]
         + [sems, sems((stages, 2))]
         + [sems, sems((stages,))] * 2,
         compiler_params=pltpu.CompilerParams(

time: 47.6 us -> 47.6 us (level)
  the two profiles are of different devices: /device:TPU:0 before, /device:TPU:9 now
where the time goes in v5:
time: 47.6 us; the launch traced here: 47.4 us
  Pallas kernels  46.7 us (98%)
  local copies, waits for them, and re-layouts  0.71 us (1%)
    pallas_call x1, Pallas kernels, fused(): pl.pallas_call(functools.partial(layer_kernel, n_ep, cap, cuts), out_shap...  46.7 us

profile of v5, /device:TPU:9, one launch (start us, length us, event | category | flops | bytes accessed | tf_op | source)
XLA Modules:
  0.0 47.4 jit_solution(11474824438216180698)
XLA Ops:
  0.0 46.7 %shard_map.73 = bf16[256,512]{1,0:T(8,128)(2,1)S(1)} custom-call(bf16[256,512]{1,0:T(8,128)(2,1)} %tok_hbm.1, s32[2,256]{1,0:T(2,128)} %bitcast.4, f32[2,256]{1,0:T(2,128)} %bitcast.5, f32[1,2048]{1,0:T(1,128)} %bitcast.3, bf16[1,2048,768]{2,1,0:T(8,128)(2,1)} %wg_ref.1, bf16[1,2048,768]{2,1,0:T(8,128)(2,1)} %wu_ref.1, bf16[1,768,2048]{2,1,0:T(8,128)(2,1)} %wd_ref.1), custom_call_target="tpu_custom_call" | custom-call | tf_op jit(solution)/shard_map/pallas_call | solution.py:485
  46.7 0.7 %copy.9 = bf16[256,512]{1,0:T(8,128)(2,1)} copy(bf16[256,512]{1,0:T(8,128)(2,1)S(1)} %shard_map.73) | data formatting | bytes 524288
